TPU v7x, 512 devices: a 4x2x32 block of a 4x8x32 slice. The times are simulated.
512 devices in a mesh: grp: 2 (over y), sp: 32 (over z), tp: 8 (over x, core).
Axes of the slice: x: 4, y: 2, z: 32, core: 2. Of those that a mesh axis runs over, the one named last changes fastest.
The devices are a block of a 4x8x32 slice.
Arguments:
- latent: bfloat16 [32768, 4096], P(('grp', 'sp', 'tp')), parts along dimension 0, may hold values from -260 to 260
- context: bfloat16 [1536, 4096], P(('grp', 'sp')), parts along dimension 0, may hold values from -6 to 6
- conditioning: bfloat16 [8192], P(('grp', 'sp')), parts along dimension 0, may hold values from -6 to 6
- norm_gain: float32 [4096], replicated, may hold values from 0.1 to 1.9
- shift_weight: bfloat16 [4096, 4096], P('sp', 'tp'), may hold values from -0.09375 to 0.09375
- scale_weight: bfloat16 [4096, 4096], P('sp', 'tp'), may hold values from -0.09375 to 0.09375
- gate_weight: bfloat16 [4096, 4096], P('sp', 'tp'), may hold values from -0.09375 to 0.09375
- query_weight: bfloat16 [4096, 1024], P(None, 'tp'), may hold values from -3 to 3
- key_weight: bfloat16 [4096, 512], P(None, 'tp'), may hold values from -3 to 3
- value_weight: bfloat16 [4096, 512], P(None, 'tp'), may hold values from -0.09375 to 0.09375
- out_weight: bfloat16 [1024, 4096], P(None, 'tp'), may hold values from -1.5 to 1.5
- sink_logit: float32 [16], P('tp'), may hold values from 3 to 7
Outputs:
- mixed: bfloat16 [32768, 4096], P(('grp', 'sp', 'tp')), parts along dimension 0
There are 2 independent parts, one for each index of `grp`. A program takes and returns all parts, laid end to end along the dimension named above; an argument that names none is the same for every part. Nothing has to cross between parts.
All inputs are finite; a program needn't handle non-finite values.
Results may differ from a plain program's by a relative error of at most 0.012.
The roundings to bfloat16 on the way count: a program that leaves them out, or rounds other values in their place, can miss the bound.
Values may be sent and summed in bfloat16 or wider, within the bound.
A program may use at most 64 MiB of HBM per device.

v0:
```python
import jax
import jax.numpy as jnp
from jax import lax
from jax.sharding import PartitionSpec as P

HEADS = 16
KV_HEADS = 8
HD = 64
GRID_W = 64
WIN = 128
epsilon = 1e-06
rope_base = 10000.0
neg_large = -1e30


def sent_to_all(value, axis):
    count = lax.axis_size(axis)
    return lax.all_to_all(
        jnp.broadcast_to(value[None], (count, *value.shape)), axis, 0, 0, tiled=True
    )


def over_copies(value, axis):
    return sent_to_all(value, axis).sum(axis=0)


def packed_total(arrays, axis):
    ends = [0]
    for a in arrays:
        ends.append(ends[-1] + a.size)
    running = over_copies(jnp.concatenate([a.ravel() for a in arrays]), axis)
    return tuple((running[b:e].reshape(a.shape) for a, b, e in zip(arrays, ends, ends[1:])))


def rows_first(arrays, axis, dims):
    turned = [jnp.moveaxis(a, dim, 0) for a, dim in zip(arrays, dims)]
    both = jnp.concatenate([t.reshape(len(t), -1) for t in turned], axis=1)
    whole, at, outs = (lax.all_gather(both, axis, axis=0, tiled=True), 0, [])
    for t, dim in zip(turned, dims):
        share = whole[:, at : at + t[0].size].reshape(-1, *t.shape[1:])
        outs.append(jnp.moveaxis(share, 0, dim))
        at += t[0].size
    return tuple(outs)


def with_halo(cells, sides, width):
    for axis, dim in sides:
        count = lax.axis_size(axis)
        ends = count - 1
        head = lax.slice_in_dim(cells, 0, width, axis=dim)
        tail = lax.slice_in_dim(cells, cells.shape[dim] - width, cells.shape[dim], axis=dim)
        cells = jnp.concatenate(
            [
                lax.ppermute(tail, axis, [(i, (i + 1) % count) for i in range(ends)]),
                cells,
                lax.ppermute(head, axis, [((i + 1) % count, i) for i in range(ends)]),
            ],
            axis=dim,
        )
    return cells


def laid_out(tiles, dim):
    shape = list(tiles.shape[1:])
    shape[dim] *= tiles.shape[0]
    return jnp.moveaxis(tiles, 0, dim).reshape(shape)


def collect(value, axis, dim):
    return laid_out(sent_to_all(value, axis), dim)


def row_norm(matrix, norm_gain):
    values = matrix.astype(jnp.float32)
    return (
        values * lax.rsqrt(jnp.mean(values * values, axis=-1, keepdims=True) + epsilon) * norm_gain
    )


def axial_turn(values, position):
    half_dim = values.shape[-1] // 2
    quarter = half_dim // 2
    inverse = rope_base ** (-jnp.arange(quarter, dtype=jnp.float32) / quarter)

    def turn(section, coordinate):
        angles = coordinate.astype(jnp.float32)[:, None] * inverse[None, :]
        cosine = jnp.cos(angles)[:, None, :]
        sine_part = jnp.sin(angles)[:, None, :]
        leading = section[..., :quarter]
        trailing = section[..., quarter:]
        return jnp.concatenate(
            [leading * cosine - trailing * sine_part, leading * sine_part + trailing * cosine],
            axis=-1,
        )

    return jnp.concatenate(
        [
            turn(values[..., :half_dim], position // GRID_W),
            turn(values[..., half_dim:], position % GRID_W),
        ],
        axis=-1,
    )


def context_pairs(context_rows, norm_gain, key_weight, value_weight):
    prepared = row_norm(context_rows, norm_gain).astype(jnp.bfloat16)
    return jnp.concatenate(
        [
            jnp.dot(prepared, key_weight, preferred_element_type=jnp.float32),
            jnp.dot(prepared, value_weight, preferred_element_type=jnp.float32),
        ],
        axis=1,
    ).astype(jnp.bfloat16)


def local(
    latent,
    context,
    conditioning,
    norm_gain,
    shift_weight,
    scale_weight,
    gate_weight,
    query_weight,
    key_weight,
    value_weight,
    out_weight,
    sink_logit,
):
    lifted = jax.nn.silu(conditioning.astype(jnp.float32)).astype(jnp.bfloat16)[None, :]
    shift_part = jnp.dot(lifted, shift_weight, preferred_element_type=jnp.float32)[0]
    scale_part = jnp.dot(lifted, scale_weight, preferred_element_type=jnp.float32)[0]
    gate_part = jnp.dot(lifted, gate_weight, preferred_element_type=jnp.float32)[0]
    summed = packed_total((shift_part, scale_part, gate_part), "sp")
    shift_vec, scale_vec, gate_vec = rows_first((summed[0], summed[1], summed[2]), "tp", (0, 0, 0))
    normed = (row_norm(latent, norm_gain) * (1.0 + scale_vec) + shift_vec).astype(jnp.bfloat16)
    segment = lax.all_gather(normed, "tp", axis=0, tiled=True)
    projected = jnp.concatenate(
        [
            jnp.dot(segment, query_weight, preferred_element_type=jnp.float32),
            jnp.dot(segment, key_weight, preferred_element_type=jnp.float32),
            jnp.dot(segment, value_weight, preferred_element_type=jnp.float32),
        ],
        axis=1,
    )
    row_count = projected.shape[0]
    query_width = query_weight.shape[1]
    key_width = key_weight.shape[1]
    query_heads = query_width // HD
    pair_heads = key_width // HD
    group_size = HEADS // KV_HEADS
    row_offset = lax.axis_index("sp") * row_count
    position = row_offset + jnp.arange(row_count, dtype=jnp.int32)
    queries = axial_turn(
        projected[:, :query_width].reshape(row_count, query_heads, HD), position
    ).astype(jnp.bfloat16)
    latent_keys = axial_turn(
        projected[:, query_width : query_width + key_width].reshape(row_count, pair_heads, HD),
        position,
    ).astype(jnp.bfloat16)
    latent_values = projected[:, query_width + key_width :].astype(jnp.bfloat16)
    key_value = jnp.concatenate([latent_keys.reshape(row_count, key_width), latent_values], axis=1)
    widened = with_halo(key_value, (("sp", 0),), WIN)
    context_all = collect(context_pairs(context, norm_gain, key_weight, value_weight), "sp", 0)
    block_count = row_count // WIN
    context_count = context_all.shape[0]
    query_blocks = queries.reshape(block_count, WIN, pair_heads, group_size, HD)
    band_blocks = widened.reshape(block_count + 2, WIN, 2 * key_width)
    band_rows = jnp.concatenate(
        [band_blocks[:block_count], band_blocks[1 : block_count + 1], band_blocks[2:]], axis=1
    )
    band_keys = band_rows[..., :key_width].reshape(block_count, 3 * WIN, pair_heads, HD)
    band_values = band_rows[..., key_width:].reshape(block_count, 3 * WIN, pair_heads, HD)
    context_keys = context_all[:, :key_width].reshape(context_count, pair_heads, HD)
    context_values = context_all[:, key_width:].reshape(context_count, pair_heads, HD)
    factor = HD ** (-0.5)
    local_scores = (
        jnp.einsum("nqhgd,nkhd->nhgqk", query_blocks, band_keys, preferred_element_type=jnp.float32)
        * factor
    )
    query_pos = position.reshape(block_count, WIN)
    key_pos = (
        row_offset
        - WIN
        + jnp.arange(block_count, dtype=jnp.int32)[:, None] * WIN
        + jnp.arange(3 * WIN, dtype=jnp.int32)[None, :]
    )
    seq_total = row_count * lax.axis_size("sp")
    allowed = (
        (jnp.abs(key_pos[:, None, :] - query_pos[:, :, None]) <= WIN)
        & (key_pos[:, None, :] >= 0)
        & (key_pos[:, None, :] < seq_total)
    )
    local_scores = jnp.where(allowed[:, None, None], local_scores, neg_large)
    context_scores = (
        jnp.einsum(
            "nqhgd,thd->nhgqt", query_blocks, context_keys, preferred_element_type=jnp.float32
        )
        * factor
    )
    sink_values = sink_logit.reshape(pair_heads, group_size)[None, :, :, None, None]
    highest = jnp.maximum(
        jnp.maximum(
            jnp.max(local_scores, axis=-1, keepdims=True),
            jnp.max(context_scores, axis=-1, keepdims=True),
        ),
        sink_values,
    )
    local_exp = jnp.exp(local_scores - highest)
    context_exp = jnp.exp(context_scores - highest)
    denominator = (
        jnp.sum(local_exp, axis=-1, keepdims=True)
        + jnp.sum(context_exp, axis=-1, keepdims=True)
        + jnp.exp(sink_values - highest)
    )
    local_weights = (local_exp / denominator).astype(jnp.bfloat16)
    context_weights = (context_exp / denominator).astype(jnp.bfloat16)
    attended = jnp.einsum(
        "nhgqk,nkhd->nqhgd", local_weights, band_values, preferred_element_type=jnp.float32
    ) + jnp.einsum(
        "nhgqt,thd->nqhgd", context_weights, context_values, preferred_element_type=jnp.float32
    )
    attended = attended.reshape(row_count, query_width).astype(jnp.bfloat16)
    columns_part = jnp.dot(
        collect(attended, "tp", 1), out_weight, preferred_element_type=jnp.float32
    ).astype(jnp.bfloat16)
    blended = lax.all_to_all(columns_part, "tp", split_axis=0, concat_axis=1, tiled=True)
    return (latent.astype(jnp.float32) + gate_vec * blended.astype(jnp.float32)).astype(
        jnp.bfloat16
    )


def solution(mesh):
    in_specs = (
        P(("grp", "sp", "tp"), None),
        P(("grp", "sp"), None),
        P(("grp", "sp")),
        P(),
        P("sp", "tp"),
        P("sp", "tp"),
        P("sp", "tp"),
        P(None, "tp"),
        P(None, "tp"),
        P(None, "tp"),
        P(None, "tp"),
        P("tp"),
    )
    out_specs = P(("grp", "sp", "tp"), None)
    return jax.shard_map(local, mesh=mesh, in_specs=in_specs, out_specs=out_specs, check_vma=False)
```

profile of v0, /device:TPU:33, one launch (start us, length us, event | category | flops | bytes accessed | tf_op | source)
XLA Modules:
  0.0 197.6 jit_solution(16965403692785830598)
XLA Ops:
  6.6 1.2 fusion.60
  7.8 1.1 fusion.58
  8.8 1.1 fusion.56
  9.9 0.8 broadcast_in_dim.14
  10.7 46.3 %all-to-all-start = ((f32[32,1,1536]{2,1,0:T(1,128)}), f32[32,1,1536]{2,1,0:T(1,128)S(1)}, u32[]{:S(2)}, u32[]{:S(2)}) async-start(f32[32,1,1536]{2,1,0:T(1,128)} %broadcast_in_dim.14), calls=%async_computation | async-start | bytes 393216 | tf_op jit(solution)/shard_map/all_to_all | solution.py:18
  57.0 0.1 all-gather.2.cloned.1.call-start
  57.1 1.2 fusion.12
  58.3 33.6 %all-to-all-done = f32[32,1,1536]{2,1,0:T(1,128)S(1)} async-done(((f32[32,1,1536]{2,1,0:T(1,128)}), f32[32,1,1536]{2,1,0:T(1,128)S(1)}, u32[]{:S(2)}, u32[]{:S(2)}) %all-to-all-start) | async-done | bytes 196640 | tf_op jit(solution)/shard_map/all_to_all | solution.py:18
  91.9 0.1 reduce_sum.45
  92.0 15.7 %all_gather.6 = f32[4096,3]{0,1:T(4,128)S(1)} all-gather(f32[512,3]{0,1:T(4,128)S(1)} %pad_maximum_fusion.3), channel_id=1, replica_groups=mesh['grp'=2,'sp'=32,'tp'=8] {'tp'}, dimensions={0}, use_global_device_ids=true | all-gather | bytes 55296 | tf_op jit(solution)/shard_map/all_gather | solution.py:38
  107.8 2.1 %fusion.16 = bf16[64,4096]{1,0:T(8,128)(2,1)} fusion(bf16[64,4096]{1,0:T(8,128)(2,1)} %param.12, f32[4096]{0:T(1024)S(1)} %bitcast.164, f32[4096]{0:T(1024)S(1)} %bitcast.165, f32[4096]{0:T(1024)} %param.15, f32[64]{0:T(128)S(1)} %add_rsqrt_fusion.1), kind=kLoop, calls=%fused_computation.29 | loop fusion | flops 1572864 | bytes 1097984 | tf_op jit(solution)/shard_map/convert_element_type | solution.py:136
  109.9 0.1 all-gather.2.cloned.1.call-update
  110.0 0.2 fusion.21
  110.2 0.3 convolution_convert_fusion.2
  110.5 0.3 convolution_convert_fusion.3
  110.8 0.1 pad_maximum_fusion.4
  110.9 0.7 broadcast_in_dim.17
  111.6 4.8 %all-to-all-start.1 = ((bf16[32,24,128]{2,1,0:T(8,128)(2,1)}), bf16[32,24,128]{2,1,0:T(8,128)(2,1)S(1)}, u32[]{:S(2)}, u32[]{:S(2)}) async-start(bf16[32,24,128]{2,1,0:T(8,128)(2,1)} %broadcast_in_dim.17), calls=%async_computation.1 | async-start | bytes 393216 | tf_op jit(solution)/shard_map/all_to_all | solution.py:18
  116.5 0.1 fusion.50
  116.5 0.1 iota_add_fusion
  116.6 0.3 multiply_cosine_fusion
  116.9 0.9 fusion.20
  117.9 21.9 %all-gather.2.cloned.1.call-done = bf16[512,4096]{1,0:T(8,128)(2,1)} async-done(((bf16[64,4096]{1,0:T(8,128)(2,1)}), bf16[512,4096]{1,0:T(8,128)(2,1)}) %all-gather.2.cloned.1.call-update) | async-done | bytes 4194320 | tf_op jit(solution)/shard_map/all_gather | solution.py:137
  139.8 3.7 %convolution_bitcast_fusion.1 = f32[512,1,64]{0,2,1:T(8,128)S(1)} fusion(bf16[512,4096]{1,0:T(8,128)(2,1)} %all-gather.2.cloned.1.call-done, bf16[4096,64]{0,1:T(8,128)(2,1)S(1)} %copy-done.3), kind=kOutput, calls=%fused_computation.20 | convolution fusion | flops 268435456 | bytes 4849664 | tf_op jit(solution)/shard_map/dot_general | solution.py:141
  143.5 0.2 constant_dynamic-update-slice_fusion.3
  143.7 0.2 constant_dynamic-update-slice_fusion.2
  143.9 0.2 constant_dynamic-update-slice_fusion.1
  144.1 0.2 constant_dynamic-update-slice_fusion
  144.3 1.4 fusion.11
  145.7 1.3 collective-permute-start.1
  147.0 4.2 %collective-permute-start = (bf16[128,128]{0,1:T(8,128)(2,1)S(1)}, bf16[128,128]{0,1:T(8,128)(2,1)S(1)}, u32[]{:S(2)}, u32[]{:S(2)}) collective-permute-start(bf16[128,128]{0,1:T(8,128)(2,1)S(1)} %get-tuple-element.14), channel_id=1, source_target_pairs={{0,8},{8,16},{16,24},{24,32},{32,40},{40,48},{48,56},{56,64},{64,7... | collective-permute-start | bytes 98312 | tf_op jit(solution)/shard_map/ppermute | solution.py:54
  151.3 1.5 fusion.70
  152.9 0.6 bitcast_reduce_fusion
  153.7 0.4 fusion.69
  154.1 0.1 maximum_maximum_fusion
  154.2 0.5 fusion.1
  154.8 0.2 fusion.5
  155.0 0.1 exponential_add_fusion
  155.1 0.8 fusion.7
  155.9 0.4 fusion.10
  156.3 0.1 copy.58
  156.4 0.1 broadcast_in_dim.18
  156.5 19.3 %all_to_all.29 = bf16[8,512,128]{1,2,0:T(8,128)(2,1)S(1)} all-to-all(bf16[8,512,128]{1,2,0:T(8,128)(2,1)S(1)} %broadcast_in_dim.18), channel_id=1, replica_groups=mesh['grp'=2,'sp'=32,'tp'=8] {'tp'}, dimensions={0} | all-to-all | bytes 2097152 | tf_op jit(solution)/shard_map/all_to_all | solution.py:18
  175.9 0.7 convolution_convert_fusion
  176.6 13.0 %all_to_all.30 = bf16[8,64,512]{2,1,0:T(8,128)(2,1)S(1)} all-to-all(bf16[8,64,512]{2,1,0:T(8,128)(2,1)S(1)} %bitcast.161), channel_id=1, replica_groups=mesh['grp'=2,'sp'=32,'tp'=8] {'tp'}, dimensions={0} | all-to-all | bytes 1048576 | tf_op jit(solution)/shard_map/all_to_all | solution.py:227
  189.6 0.1 convert_bitcast_fusion
  189.7 0.1 copy.79
  189.8 0.9 fusion.17
  (42 shorter events, 0.5 us)
Async XLA Ops:
  6.5 169.3 %copy-start = (bf16[1024,512]{1,0:T(8,128)(2,1)S(1)}, bf16[1024,512]{1,0:T(8,128)(2,1)}, u32[]{:S(2)}) copy-start(bf16[1024,512]{1,0:T(8,128)(2,1)} %param.22) | copy-start | bytes 3145732
  6.6 103.6 %copy-start.7 = (f32[4096]{0:T(1024)S(1)}, f32[4096]{0:T(1024)}, u32[]{:S(2)}) copy-start(f32[4096]{0:T(1024)} %param.15) | copy-start | bytes 49156
  6.6 103.4 %copy-start.5 = (bf16[24,4096]{1,0:T(8,128)(2,1)S(1)}, bf16[24,4096]{1,0:T(8,128)(2,1)}, u32[]{:S(2)}) copy-start(bf16[24,4096]{1,0:T(8,128)(2,1)} %param.13) | copy-start | bytes 589828
  6.6 103.6 %copy-start.4 = (bf16[4096,64]{0,1:T(8,128)(2,1)S(1)}, bf16[4096,64]{0,1:T(8,128)(2,1)}, u32[]{:S(2)}) copy-start(bf16[4096,64]{0,1:T(8,128)(2,1)} %param.21) | copy-start | bytes 1572868
  6.6 103.9 %copy-start.3 = (bf16[4096,64]{0,1:T(8,128)(2,1)S(1)}, bf16[4096,64]{0,1:T(8,128)(2,1)}, u32[]{:S(2)}) copy-start(bf16[4096,64]{0,1:T(8,128)(2,1)} %param.20) | copy-start | bytes 1572868
  10.7 81.2 %all-to-all-start = ((f32[32,1,1536]{2,1,0:T(1,128)}), f32[32,1,1536]{2,1,0:T(1,128)S(1)}, u32[]{:S(2)}, u32[]{:S(2)}) async-start(f32[32,1,1536]{2,1,0:T(1,128)} %broadcast_in_dim.14), calls=%async_computation | async-start | bytes 393216 | tf_op jit(solution)/shard_map/all_to_all | solution.py:18
  57.0 82.8 %all-gather.2.cloned.1.call-start = ((), (), s32[]{:S(2)}) async-start(), calls=%async_computation.4 | async-start | bytes 4718592 | tf_op jit(solution)/shard_map/all_gather | solution.py:137
  111.6 41.3 %all-to-all-start.1 = ((bf16[32,24,128]{2,1,0:T(8,128)(2,1)}), bf16[32,24,128]{2,1,0:T(8,128)(2,1)S(1)}, u32[]{:S(2)}, u32[]{:S(2)}) async-start(bf16[32,24,128]{2,1,0:T(8,128)(2,1)} %broadcast_in_dim.17), calls=%async_computation.1 | async-start | bytes 393216 | tf_op jit(solution)/shard_map/all_to_all | solution.py:18
  139.8 4.5 %copy-start.1 = (bf16[512,4096]{1,0:T(8,128)(2,1)S(1)}, bf16[512,4096]{1,0:T(8,128)(2,1)}, u32[]{:S(2)}) copy-start(bf16[512,4096]{1,0:T(8,128)(2,1)} %all-gather.2.cloned.1.call-done) | copy-start | bytes 12582916
  143.5 7.8 %copy-start.6 = (bf16[4096,128]{1,0:T(8,128)(2,1)S(1)}, bf16[4096,128]{1,0:T(8,128)(2,1)}, u32[]{:S(2)}) copy-start(bf16[4096,128]{1,0:T(8,128)(2,1)} %param.19) | copy-start | bytes 3145732
  145.7 7.8 %collective-permute-start.1 = (bf16[128,128]{0,1:T(8,128)(2,1)S(1)}, bf16[128,128]{0,1:T(8,128)(2,1)S(1)}, u32[]{:S(2)}, u32[]{:S(2)}) collective-permute-start(bf16[128,128]{0,1:T(8,128)(2,1)S(1)} %get-tuple-element.13), channel_id=1, source_target_pairs={{8,0},{16,8},{24,16},{32,24},{40,32},{48,40},{56,48},{64,56},{72,6... | collective-permute-start | bytes 98312 | tf_op jit(solution)/shard_map/ppermute | solution.py:56
  147.0 6.5 %collective-permute-start = (bf16[128,128]{0,1:T(8,128)(2,1)S(1)}, bf16[128,128]{0,1:T(8,128)(2,1)S(1)}, u32[]{:S(2)}, u32[]{:S(2)}) collective-permute-start(bf16[128,128]{0,1:T(8,128)(2,1)S(1)} %get-tuple-element.14), channel_id=1, source_target_pairs={{0,8},{8,16},{16,24},{24,32},{32,40},{40,48},{48,56},{56,64},{64,7... | collective-permute-start | bytes 98312 | tf_op jit(solution)/shard_map/ppermute | solution.py:54
  152.9 1.2 copy-start.8
  176.6 13.2 %copy-start.2 = (bf16[64,4096]{1,0:T(8,128)(2,1)S(1)}, bf16[64,4096]{1,0:T(8,128)(2,1)}, u32[]{:S(2)}) copy-start(bf16[64,4096]{1,0:T(8,128)(2,1)} %param.12) | copy-start | bytes 1572868
Sparse Core Ops, SparseCore 0:
  110.1 29.6 all-gather.1
where the time goes:
time: 198 us
  starting transfers between devices  56.7 us (29%)
  waiting for transfers between devices  55.5 us (28%)
  blocking collectives  48 us (24%)
  between operations  13.8 us (7%)
  matrix products  13.5 us (7%)
  other arithmetic  8.05 us (4%)
  local copies, waits for them, and re-layouts  2.02 us (1%)
    all_to_all x2, starting transfers between devices, sent_to_all(): lax.all_to_all(jnp.broadcast_to(value[None], (count, *value.shape)), axis...  51.1 us
    all_to_all x2, waiting for transfers between devices, sent_to_all(): lax.all_to_all(jnp.broadcast_to(value[None], (count, *value.shape)), axis...  33.6 us
    all_gather x1, waiting for transfers between devices, local(): segment = lax.all_gather(normed, 'tp', axis=0, tiled=True)  21.9 us
    all_to_all x1, blocking collectives, sent_to_all(): lax.all_to_all(jnp.broadcast_to(value[None], (count, *value.shape)), axis...  19.3 us
    all_gather x1, blocking collectives, rows_first(): whole, at, outs = (lax.all_gather(both, axis, axis=0, tiled=True), 0, [])  15.7 us
    all_to_all x1, blocking collectives, local(): lax.all_to_all(columns_part, 'tp', split_axis=0, concat_axis=1, tiled=True)  13 us
    ppermute x1, starting transfers between devices, with_halo(): lax.ppermute(tail, axis, [(i, (i + 1) % count) for i in range(ends)])  4.21 us
  transfers between devices with their start and end apart: 5, of which 2 were waited for; matrix products, arithmetic and copies ran while one was open for 6% of the time, Pallas kernels for 0%

commit v1 on v0

--- a/solution.py
+++ b/solution.py
@@ -2,6 +2,7 @@
 import jax.numpy as jnp
 from jax import lax
 from jax.sharding import PartitionSpec as P
+from jax.lax import all_to_all, axis_size
 
 HEADS = 16
 KV_HEADS = 8
@@ -11,6 +12,18 @@
 epsilon = 1e-06
 rope_base = 10000.0
 neg_large = -1e30
+
+
+def link_files(unit, device_axis):
+    return jnp.concatenate(
+        all_to_all(
+            jnp.stack([unit for _ in range(axis_size(device_axis))], axis=0),
+            axis_name=device_axis,
+            split_axis=0,
+            concat_axis=0,
+        ),
+        axis=0,
+    )
 
 
 def sent_to_all(value, axis):
@@ -134,7 +147,7 @@
     summed = packed_total((shift_part, scale_part, gate_part), "sp")
     shift_vec, scale_vec, gate_vec = rows_first((summed[0], summed[1], summed[2]), "tp", (0, 0, 0))
     normed = (row_norm(latent, norm_gain) * (1.0 + scale_vec) + shift_vec).astype(jnp.bfloat16)
-    segment = lax.all_gather(normed, "tp", axis=0, tiled=True)
+    segment = link_files(normed, "tp")
     projected = jnp.concatenate(
         [
             jnp.dot(segment, query_weight, preferred_element_type=jnp.float32),

time: 198 us -> 238 us (1.20)
  waiting for transfers between devices: 55.5 us -> 97.3 us
  between operations: 13.8 us -> 0.37 us
  matrix products: 13.5 us -> 17.7 us
  local copies, waits for them, and re-layouts: 2.02 us -> 5.89 us
  starting transfers between devices: 56.7 us -> 59.7 us
    all_to_all x0 -> x1, waiting for transfers between devices: none -> 45.1 us  [link_files(): all_to_all(jnp.stack([unit for _ in range(axis_size(device_axis))], axis=...]
    all_gather x1 -> x0, waiting for transfers between devices: 21.9 us -> none  [local(): segment = lax.all_gather(normed, 'tp', axis=0, tiled=True)]
    all_to_all x2, waiting for transfers between devices: 33.6 us -> 52.2 us  [sent_to_all(): lax.all_to_all(jnp.broadcast_to(value[None], (count, *value.shape)), axis...]
    all_to_all x0 -> x1, starting transfers between devices: none -> 4.75 us  [link_files(): all_to_all(jnp.stack([unit for _ in range(axis_size(device_axis))], axis=...]
    another operation x0 -> x1, local copies, waits for them, and re-layouts: none -> 2.5 us  [link_files(): jnp.stack([unit for _ in range(axis_size(device_axis))], axis=0)]
  transfers between devices with their start and end apart: 5 -> 5, of which waited for: 2 -> 3; matrix products, arithmetic and copies ran while one was open for 6% -> 7% of each run, Pallas kernels for 0% -> 0%
where the time goes in v1:
time: 238 us
  waiting for transfers between devices  97.3 us (41%)
  starting transfers between devices  59.7 us (25%)
  blocking collectives  49.4 us (21%)
  matrix products  17.7 us (7%)
  other arithmetic  7.25 us (3%)
  local copies, waits for them, and re-layouts  5.89 us (2%)
    all_to_all x2, waiting for transfers between devices, sent_to_all(): lax.all_to_all(jnp.broadcast_to(value[None], (count, *value.shape)), axis...  52.2 us
    all_to_all x2, starting transfers between devices, sent_to_all(): lax.all_to_all(jnp.broadcast_to(value[None], (count, *value.shape)), axis...  51.1 us
    all_to_all x1, waiting for transfers between devices, link_files(): all_to_all(jnp.stack([unit for _ in range(axis_size(device_axis))], axis=...  45.1 us
    all_to_all x1, blocking collectives, sent_to_all(): lax.all_to_all(jnp.broadcast_to(value[None], (count, *value.shape)), axis...  20.7 us
    all_gather x1, blocking collectives, rows_first(): whole, at, outs = (lax.all_gather(both, axis, axis=0, tiled=True), 0, [])  15.7 us
    all_to_all x1, blocking collectives, local(): lax.all_to_all(columns_part, 'tp', split_axis=0, concat_axis=1, tiled=True)  13 us
  transfers between devices with their start and end apart: 5, of which 3 were waited for; matrix products, arithmetic and copies ran while one was open for 7% of the time, Pallas kernels for 0%

profile of v1, /device:TPU:33, one launch (start us, length us, event | category | flops | bytes accessed | tf_op | source)
XLA Modules:
  0.0 237.6 jit_solution(15978489735749285395)
XLA Ops:
  0.0 1.1 fusion.60
  1.1 1.1 fusion.58
  2.2 1.1 fusion.56
  3.3 0.8 broadcast_in_dim.14
  4.1 46.3 %all-to-all-start = ((f32[32,1,1536]{2,1,0:T(1,128)}), f32[32,1,1536]{2,1,0:T(1,128)S(1)}, u32[]{:S(2)}, u32[]{:S(2)}) async-start(f32[32,1,1536]{2,1,0:T(1,128)} %broadcast_in_dim.14), calls=%async_computation | async-start | bytes 393216 | tf_op jit(solution)/shard_map/all_to_all | solution.py:31
  50.4 1.2 fusion.12
  51.6 33.6 %all-to-all-done = f32[32,1,1536]{2,1,0:T(1,128)S(1)} async-done(((f32[32,1,1536]{2,1,0:T(1,128)}), f32[32,1,1536]{2,1,0:T(1,128)S(1)}, u32[]{:S(2)}, u32[]{:S(2)}) %all-to-all-start) | async-done | bytes 196640 | tf_op jit(solution)/shard_map/all_to_all | solution.py:31
  85.3 0.1 reduce_sum.45
  85.4 15.7 %all_gather.3 = f32[4096,3]{0,1:T(4,128)S(1)} all-gather(f32[512,3]{0,1:T(4,128)S(1)} %pad_maximum_fusion.3), channel_id=1, replica_groups=mesh['grp'=2,'sp'=32,'tp'=8] {'tp'}, dimensions={0}, use_global_device_ids=true | all-gather | bytes 55296 | tf_op jit(solution)/shard_map/all_gather | solution.py:51
  101.2 1.3 fusion.16
  102.5 2.5 %stack.2 = bf16[8,64,4096]{2,1,0:T(8,128)(2,1)} broadcast(bf16[64,4096]{1,0:T(8,128)(2,1)S(1)} %fusion.16), dimensions={1,2} | broadcast | bytes 4718592 | tf_op jit(solution)/shard_map/stack | solution.py:20
  105.0 4.8 %all-to-all-start.1 = ((bf16[8,64,4096]{2,1,0:T(8,128)(2,1)}), bf16[8,64,4096]{2,1,0:T(8,128)(2,1)}, u32[]{:S(2)}, u32[]{:S(2)}) async-start(bf16[8,64,4096]{2,1,0:T(8,128)(2,1)} %stack.2), calls=%async_computation.1 | async-start | bytes 8388608 | tf_op jit(solution)/shard_map/all_to_all | solution.py:19
  109.8 1.4 copy.57
  111.2 0.2 fusion.21
  111.4 0.3 convolution_convert_fusion.2
  111.7 0.3 convolution_convert_fusion.3
  112.1 0.1 pad_maximum_fusion.4
  112.1 0.1 fusion.50
  112.3 0.3 multiply_cosine_fusion
  112.6 0.9 fusion.20
  113.6 45.1 %all-to-all-done.1 = bf16[8,64,4096]{2,1,0:T(8,128)(2,1)} async-done(((bf16[8,64,4096]{2,1,0:T(8,128)(2,1)}), bf16[8,64,4096]{2,1,0:T(8,128)(2,1)}, u32[]{:S(2)}, u32[]{:S(2)}) %all-to-all-start.1) | async-done | bytes 4194336 | tf_op jit(solution)/shard_map/all_to_all | solution.py:19
  158.7 0.7 broadcast_in_dim.17
  159.4 4.8 %all-to-all-start.2 = ((bf16[32,24,128]{2,1,0:T(8,128)(2,1)}), bf16[32,24,128]{2,1,0:T(8,128)(2,1)S(1)}, u32[]{:S(2)}, u32[]{:S(2)}) async-start(bf16[32,24,128]{2,1,0:T(8,128)(2,1)} %broadcast_in_dim.17), calls=%async_computation.2 | async-start | bytes 393216 | tf_op jit(solution)/shard_map/all_to_all | solution.py:31
  164.1 3.6 %convolution_bitcast_fusion.1 = f32[512,1,64]{0,2,1:T(8,128)S(1)} fusion(bf16[512,4096]{1,0:T(8,128)(2,1)} %bitcast.12, bf16[4096,64]{0,1:T(8,128)(2,1)S(1)} %copy-done.2), kind=kOutput, calls=%fused_computation.20 | convolution fusion | flops 268435456 | bytes 4849664 | tf_op jit(solution)/shard_map/dot_general | solution.py:154
  167.7 0.2 constant_dynamic-update-slice_fusion.3
  167.9 0.2 constant_dynamic-update-slice_fusion.2
  168.1 0.2 constant_dynamic-update-slice_fusion.1
  168.3 0.2 constant_dynamic-update-slice_fusion
  168.5 3.6 %fusion.11 = bf16[512,128]{0,1:T(8,128)(2,1)S(1)} fusion(bf16[512,128]{0,1:T(8,128)(2,1)S(1)} %constant_dynamic-update-slice_fusion, bf16[512,4096]{1,0:T(8,128)(2,1)} %bitcast.12, bf16[4096,64]{0,1:T(8,128)(2,1)S(1)} %copy-done.3), kind=kOutput, calls=%fused_computation.22 | convolution fusion | flops 268468224 | bytes 4784128 | tf_op jit(solution)/shard_map/dot_general | solution.py:155
  172.1 2.4 collective-permute-start
  174.5 1.5 collective-permute-start.1
  176.0 3.7 %fusion.70 = f32[512,2,64]{0,2,1:T(8,128)S(1)} fusion(bf16[512,4096,1]{1,0,2:T(8,128)(2,1)} %bitcast.22, bf16[2,64,4096]{2,1,0:T(8,128)(2,1)S(1)} %bitcast.161), kind=kOutput, calls=%fused_computation.135 | convolution fusion | flops 536870912 | bytes 5505024 | tf_op jit(solution)/shard_map/dot_general | solution.py:153
  179.9 18.6 %all-to-all-done.2 = bf16[32,24,128]{2,1,0:T(8,128)(2,1)S(1)} async-done(((bf16[32,24,128]{2,1,0:T(8,128)(2,1)}), bf16[32,24,128]{2,1,0:T(8,128)(2,1)S(1)}, u32[]{:S(2)}, u32[]{:S(2)}) %all-to-all-start.2) | async-done | bytes 196640 | tf_op jit(solution)/shard_map/all_to_all | solution.py:31
  198.4 0.6 bitcast_reduce_fusion
  199.2 0.4 fusion.69
  199.7 0.5 fusion.1
  200.2 0.2 fusion.5
  200.5 0.1 exponential_add_fusion
  200.6 0.8 fusion.7
  201.4 0.4 fusion.10
  201.8 0.1 copy.66
  201.9 0.1 broadcast_in_dim.18
  202.0 20.7 %all_to_all.34 = bf16[8,512,128]{1,2,0:T(8,128)(2,1)S(1)} all-to-all(bf16[8,512,128]{1,2,0:T(8,128)(2,1)S(1)} %broadcast_in_dim.18), channel_id=1, replica_groups=mesh['grp'=2,'sp'=32,'tp'=8] {'tp'}, dimensions={0} | all-to-all | bytes 2097152 | tf_op jit(solution)/shard_map/all_to_all | solution.py:31
  222.7 0.7 convolution_convert_fusion
  223.5 13.0 %all_to_all.35 = bf16[8,64,512]{2,1,0:T(8,128)(2,1)S(1)} all-to-all(bf16[8,64,512]{2,1,0:T(8,128)(2,1)S(1)} %bitcast.166), channel_id=1, replica_groups=mesh['grp'=2,'sp'=32,'tp'=8] {'tp'}, dimensions={0} | all-to-all | bytes 1048576 | tf_op jit(solution)/shard_map/all_to_all | solution.py:240
  236.4 0.1 convert_bitcast_fusion
  236.6 0.1 copy.87
  236.7 0.9 fusion.17
  (43 shorter events, 0.6 us)
Async XLA Ops:
  0.0 222.7 %copy-start = (bf16[1024,512]{1,0:T(8,128)(2,1)S(1)}, bf16[1024,512]{1,0:T(8,128)(2,1)}, u32[]{:S(2)}) copy-start(bf16[1024,512]{1,0:T(8,128)(2,1)} %param.22) | copy-start | bytes 3145732
  4.1 81.2 %all-to-all-start = ((f32[32,1,1536]{2,1,0:T(1,128)}), f32[32,1,1536]{2,1,0:T(1,128)S(1)}, u32[]{:S(2)}, u32[]{:S(2)}) async-start(f32[32,1,1536]{2,1,0:T(1,128)} %broadcast_in_dim.14), calls=%async_computation | async-start | bytes 393216 | tf_op jit(solution)/shard_map/all_to_all | solution.py:31
  105.0 4.8 %copy-start.5 = (bf16[4096,128]{1,0:T(8,128)(2,1)S(1)}, bf16[4096,128]{1,0:T(8,128)(2,1)}, u32[]{:S(2)}) copy-start(bf16[4096,128]{1,0:T(8,128)(2,1)} %param.19) | copy-start | bytes 3145732
  105.0 6.2 %copy-start.4 = (bf16[24,4096]{1,0:T(8,128)(2,1)S(1)}, bf16[24,4096]{1,0:T(8,128)(2,1)}, u32[]{:S(2)}) copy-start(bf16[24,4096]{1,0:T(8,128)(2,1)} %param.13) | copy-start | bytes 589828
  105.0 6.4 %copy-start.3 = (bf16[4096,64]{0,1:T(8,128)(2,1)S(1)}, bf16[4096,64]{0,1:T(8,128)(2,1)}, u32[]{:S(2)}) copy-start(bf16[4096,64]{0,1:T(8,128)(2,1)} %param.21) | copy-start | bytes 1572868
  105.0 6.4 %copy-start.7 = (f32[4096]{0:T(1024)S(1)}, f32[4096]{0:T(1024)}, u32[]{:S(2)}) copy-start(f32[4096]{0:T(1024)} %param.15) | copy-start | bytes 49156
  105.0 6.7 %copy-start.2 = (bf16[4096,64]{0,1:T(8,128)(2,1)S(1)}, bf16[4096,64]{0,1:T(8,128)(2,1)}, u32[]{:S(2)}) copy-start(bf16[4096,64]{0,1:T(8,128)(2,1)} %param.20) | copy-start | bytes 1572868
  105.0 53.6 %all-to-all-start.1 = ((bf16[8,64,4096]{2,1,0:T(8,128)(2,1)}), bf16[8,64,4096]{2,1,0:T(8,128)(2,1)}, u32[]{:S(2)}, u32[]{:S(2)}) async-start(bf16[8,64,4096]{2,1,0:T(8,128)(2,1)} %stack.2), calls=%async_computation.1 | async-start | bytes 8388608 | tf_op jit(solution)/shard_map/all_to_all | solution.py:19
  159.4 39.1 %all-to-all-start.2 = ((bf16[32,24,128]{2,1,0:T(8,128)(2,1)}), bf16[32,24,128]{2,1,0:T(8,128)(2,1)S(1)}, u32[]{:S(2)}, u32[]{:S(2)}) async-start(bf16[32,24,128]{2,1,0:T(8,128)(2,1)} %broadcast_in_dim.17), calls=%async_computation.2 | async-start | bytes 393216 | tf_op jit(solution)/shard_map/all_to_all | solution.py:31
  167.7 8.3 %copy-start.6 = (bf16[4096,128]{0,1:T(8,128)(2,1)S(1)}, bf16[4096,128]{0,1:T(8,128)(2,1)}, u32[]{:S(2)}) copy-start(bf16[4096,128]{0,1:T(8,128)(2,1)} %copy.57) | copy-start | bytes 3145732
  172.1 26.9 %collective-permute-start = (bf16[128,128]{0,1:T(8,128)(2,1)S(1)}, bf16[128,128]{0,1:T(8,128)(2,1)S(1)}, u32[]{:S(2)}, u32[]{:S(2)}) collective-permute-start(bf16[128,128]{0,1:T(8,128)(2,1)S(1)} %get-tuple-element.14), channel_id=1, source_target_pairs={{0,8},{8,16},{16,24},{24,32},{32,40},{40,48},{48,56},{56,64},{64,7... | collective-permute-start | bytes 98312 | tf_op jit(solution)/shard_map/ppermute | solution.py:67
  174.5 24.5 %collective-permute-start.1 = (bf16[128,128]{0,1:T(8,128)(2,1)S(1)}, bf16[128,128]{0,1:T(8,128)(2,1)S(1)}, u32[]{:S(2)}, u32[]{:S(2)}) collective-permute-start(bf16[128,128]{0,1:T(8,128)(2,1)S(1)} %get-tuple-element.13), channel_id=1, source_target_pairs={{8,0},{16,8},{24,16},{32,24},{40,32},{48,40},{56,48},{64,56},{72,6... | collective-permute-start | bytes 98312 | tf_op jit(solution)/shard_map/ppermute | solution.py:69
  198.4 1.2 copy-start.8
  223.4 13.2 %copy-start.1 = (bf16[64,4096]{1,0:T(8,128)(2,1)S(1)}, bf16[64,4096]{1,0:T(8,128)(2,1)}, u32[]{:S(2)}) copy-start(bf16[64,4096]{1,0:T(8,128)(2,1)} %param.12) | copy-start | bytes 1572868
